TPU v7x, 32 devices: a whole 2x2x4 slice. The times are simulated.
32 devices in a mesh: fs: 8 (over z, y), tp: 4 (over x, core).
Axes of the slice: x: 2, y: 2, z: 4, core: 2. Of those that a mesh axis runs over, the one named last changes fastest.
Arguments:
- mixed: bfloat16 [12288, 2048], P(('fs', 'tp')), may hold values from -6 to 6
- residual: bfloat16 [12288, 2048], P(('fs', 'tp')), may hold values from -6 to 6
- mix_weight: bfloat16 [2048, 2048], P(('fs', 'tp')), may hold values from -0.125 to 0.125
- norm_gain: float32 [2048], replicated, may hold values from 0.1 to 1.9
- up_weight: bfloat16 [2048, 5504], P('fs', 'tp'), may hold values from -0.125 to 0.125
- gate_weight: bfloat16 [2048, 5504], P('fs', 'tp'), may hold values from -0.125 to 0.125
- conv_weight: float32 [3, 5504], P(None, 'tp'), may hold values from -3 to 3
- conv_bias: float32 [5504], P('tp'), may hold values from -3 to 3
- down_weight: bfloat16 [5504, 2048], P('tp', 'fs'), may hold values from -0.078125 to 0.078125
Outputs:
- output: bfloat16 [12288, 2048], P(('fs', 'tp'))
All inputs are finite; a program needn't handle non-finite values.
Results may differ from a plain program's by a relative error of at most 0.012.
Values may be sent and summed in bfloat16 or wider, within the bound.
A program may use at most 128 MiB of HBM per device.

v0:
```python
import functools

import jax
import jax.numpy as jnp
from jax import lax
from jax.experimental import pallas as pl
from jax.experimental.pallas import tpu as pltpu
from jax.sharding import PartitionSpec as P

norm_eps = 1e-06
f32, bf16 = jnp.float32, jnp.bfloat16
MESH = pl.DeviceIdType.MESH
NT = (((1,), (1,)), ((), ()))
TILE = 256


def mod(a, n):
    return lax.rem(a + n, n)


def ring_place(f, nz, ny):
    z, y = lax.div(f, ny), lax.rem(f, ny)
    if ny == 1:
        return z
    along = jnp.where(lax.rem(z, 2) == 0, y - 1, ny - 1 - y)
    return jnp.where(y == 0, nz * (ny - 1) + nz - 1 - z, z * (ny - 1) + along)


def ring_chip(r, nz, ny):
    if ny == 1:
        return r
    z, k = lax.div(r, ny - 1), lax.rem(r, ny - 1)
    out = z * ny + jnp.where(lax.rem(z, 2) == 0, 1 + k, ny - 1 - k)
    return jnp.where(r < nz * (ny - 1), out, (nz - 1 - (r - nz * (ny - 1))) * ny)


def layer_kernel(
    nz,
    ny,
    nx,
    mixed,
    residual,
    mix_shard,
    up_shard,
    gate_shard,
    down_shard,
    gain,
    taps,
    bias,
    out,
    mix_full,
    up_full,
    gate_full,
    down_full,
    tokens,
    up_part,
    hidden,
    mixed_v,
    held,
    stream,
    keep,
    got_core,
    got_x,
    w_send,
    w_recv,
    mr_send,
    m_recv,
    mx_send,
    mc_send,
    t_recv,
    tx_send,
    tc_send,
    pc_send,
    pc_recv,
    px_send,
    px_recv,
    in_sem,
    out_sem,
):
    n = nz * ny
    half_n = n // 2
    n_tp = 2 * nx
    me = lax.axis_index("fs")
    tp = lax.axis_index("tp")
    x, core = lax.div(tp, 2), lax.rem(tp, 2)
    place = ring_place(me, nz, ny)

    def ring(d):
        return ring_chip(mod(place + d, n), nz, ny)

    nxt, prv = ring(1), ring(-1)
    twin = tp + 1 - 2 * core

    def x_at(dx):
        return lax.rem(x + dx, nx) * 2 + core

    tok, width = stream.shape
    hid, wide = up_shard.shape
    cut = (hid // 2 + 15) // 16 * 16
    halves = ((0, cut), (cut, hid - cut))
    fulls = (up_full, gate_full, down_full)
    shards = (up_shard, gate_shard, down_shard)
    n_step = n - 3
    mrows = mix_shard.shape[0]

    def remote(src, dst, send, recv, axis, to):
        return pltpu.make_async_remote_copy(
            src_ref=src,
            dst_ref=dst,
            send_sem=send,
            recv_sem=recv,
            device_id={axis: to},
            device_id_type=MESH,
        )

    def slot(m, f, h):
        off, size = halves[h]
        return fulls[m].at[pl.ds(off, size), pl.ds(pl.multiple_of(f * wide, 128), wide)]

    def w_copy(m, f, h, way, mine=False):
        off, size = halves[h]
        src = shards[m].at[pl.ds(off, size), :] if mine else slot(m, f, h)
        to = prv if way else nxt
        return remote(src, slot(m, f, h), w_send.at[m, way, f, h], w_recv.at[m, f, h], "fs", to)

    def w_own(m):
        for k in range(2):
            w_copy(m, me, k, 0, True).start()
            w_copy(m, me, 1 - k, 1, True).start()

    def w_step(m, k):
        d, h = 1 + k // 2, k % 2
        for way, f, hh in ((0, ring(-d), h), (1, ring(d), 1 - h)):
            w_copy(m, f, hh, way).wait_recv()
            if k < n_step:
                w_copy(m, f, hh, way).start()

    def w_drain(m):
        for h in range(2):
            for way in range(2):
                w_copy(m, me, h, way, True).wait_send()
        for k in range(n_step):
            d, h = 1 + k // 2, k % 2
            w_copy(m, ring(-d), h, 0).wait_send()
            w_copy(m, ring(d), 1 - h, 1).wait_send()

    def w_local(m):
        cols = pl.ds(pl.multiple_of(me * wide, 128), wide)
        return pltpu.make_async_copy(shards[m], fulls[m].at[:, cols], in_sem.at[m])

    def part(f, t):
        return mix_full.at[pl.ds(pl.multiple_of((f * n_tp + t) * mrows, 16), mrows), :]

    def m_ring(f, way, mine=False):
        src = mix_shard if mine else part(f, tp)
        to = prv if way else nxt
        return remote(src, part(f, tp), mr_send.at[way, f], m_recv.at[f, tp], "fs", to)

    def m_x(f, dx, mine=False):
        src = mix_shard if mine else part(f, tp)
        return remote(src, part(f, tp), mx_send.at[f, dx - 1], m_recv.at[f, tp], "tp", x_at(dx))

    def m_core(f, dx, mine=False):
        t = x_at(dx)
        src = mix_shard if mine else part(f, t)
        return remote(src, part(f, t), mc_send.at[f, dx], m_recv.at[f, t], "tp", twin)

    def m_spread(f, mine=False):
        for dx in range(1, nx):
            m_x(f, dx, mine).start()
        m_core(f, 0, mine).start()

    def m_wait(f, t):
        remote(part(f, t), part(f, t), mc_send.at[f, 0], m_recv.at[f, t], "tp", twin).wait_recv()

    def m_step(d):
        for way in range(2):
            if d < half_n + 1 - way:
                f = ring(d if way else -d)
                m_wait(f, tp)
                if d < half_n - way:
                    m_ring(f, way).start()
                m_spread(f)

    def m_relay(f):
        for dx in range(1, nx):
            m_wait(f, x_at(dx))
            m_core(f, dx).start()

    def m_drain():
        for q in range(n):
            d = (q + 1) // 2
            f = ring(-d if q % 2 else d)
            mine = q == 0
            for way in range(2):
                if d < half_n - way and (mine or (q % 2 == 1) == (way == 0)):
                    m_ring(f, way, mine).wait_send()
            for dx in range(1, nx):
                m_x(f, dx, mine).wait_send()
            for dx in range(nx):
                m_core(f, dx, mine and dx == 0).wait_send()

    def rows(b):
        return pl.ds(pl.multiple_of(b * tok, 16), tok)

    def t_copy(b, send, to):
        return remote(tokens.at[rows(b), :], tokens.at[rows(b), :], send, t_recv.at[b], "tp", to)

    def t_wait(b):
        t_copy(b, tc_send.at[0], twin).wait_recv()

    def columns(f):
        return pl.ds(pl.multiple_of(f * wide, 128), wide)

    def gone(dx, q):
        return mix_full.at[pl.ds(dx * tok, tok), columns(q)]

    def pc_copy(dx, q):
        return remote(
            gone(dx, q), got_core.at[dx, q], pc_send.at[q, dx], pc_recv.at[q, dx], "tp", twin
        )

    def px_copy(dx, q):
        return remote(
            keep.at[dx, q],
            got_x.at[dx - 1, q],
            px_send.at[q, dx - 1],
            px_recv.at[q, dx - 1],
            "tp",
            x_at(dx),
        )

    def out_copy(f, q):
        return pltpu.make_async_copy(held.at[:, columns(f)], out.at[:, columns(f)], out_sem.at[q])

    load_mixed = pltpu.make_async_copy(mixed, mixed_v, in_sem.at[3])
    load_residual = pltpu.make_async_copy(residual, held, in_sem.at[4])
    load_mix = pltpu.make_async_copy(mix_shard, part(me, tp), in_sem.at[5])

    barrier = pltpu.get_barrier_semaphore()
    for other in (nxt, prv):
        pl.semaphore_signal(barrier, inc=1, device_id={"fs": other}, device_id_type=MESH)
    for other in [twin] + [x_at(dx) for dx in range(1, nx)]:
        pl.semaphore_signal(barrier, inc=1, device_id={"tp": other}, device_id_type=MESH)
    pl.semaphore_wait(barrier, 2 + nx)

    m_ring(me, 0, True).start()
    m_ring(me, 1, True).start()
    m_spread(me, True)
    load_mix.start()
    load_mixed.start()
    load_residual.start()
    w_own(0)
    for m in range(3):
        w_local(m).start()
    up_part[0:16, :] = jnp.zeros((16, hid), bf16)

    early = min(n_step, half_n - 1)
    for d in range(1, half_n + 1):
        m_step(d)
        if 2 <= d < early + 2:
            w_step(0, d - 2)
    for q in range(n):
        d = (q + 1) // 2
        m_relay(ring(-d if q % 2 else d))
    for f in range(n):
        for dx in range(nx):
            m_wait(f, x_at(dx) + 1 - 2 * core)
    load_mix.wait()
    load_mixed.wait()
    load_residual.wait()

    def project(i, _):
        cols = pl.ds(pl.multiple_of(i * TILE, 128), TILE)
        made = jnp.dot(mixed_v[...], mix_full[:, cols], preferred_element_type=f32)
        stream[:, cols] = (held[:, cols].astype(f32) + made).astype(bf16)
        return 0

    lax.fori_loop(0, width // TILE, project, 0)

    for k in range(early, min(early + 1, n_step)):
        w_step(0, k)

    def norm(i, _):
        at = pl.multiple_of(i * 32, 16)
        row = stream[pl.ds(at, 32), :].astype(f32)
        scale = lax.rsqrt(jnp.mean(row * row, axis=-1, keepdims=True) + norm_eps)
        tokens[pl.ds(pl.multiple_of(tp * tok + at, 16), 32), :] = (row * scale * gain[...]).astype(
            bf16
        )
        return 0

    lax.fori_loop(0, tok // 32, norm, 0)
    for dx in range(1, nx):
        t_copy(tp, tx_send.at[dx - 1], x_at(dx)).start()
    t_copy(tp, tc_send.at[0], twin).start()

    for k in range(min(early + 1, n_step), n_step):
        w_step(0, k)
    w_own(1)
    for k in range(n_step, n - 1):
        w_step(0, k)
    w_local(0).wait()

    def block_of(j):
        return lax.rem(x + lax.div(j, 2), nx) * 2 + lax.rem(core + lax.rem(j, 2), 2)

    def up_block(j, _):
        b = block_of(j)

        @pl.when(j > 0)
        def _():
            t_wait(b)

        @pl.when((j > 1) & (lax.rem(j, 2) == 0))
        def _():
            t_copy(b, tc_send.at[lax.div(j, 2)], twin).start()

        for lo in range(0, hid, TILE):
            hi = min(lo + TILE, hid)
            made = lax.dot_general(
                tokens[rows(b), :], up_full[lo:hi, :], NT, preferred_element_type=f32
            )
            up_part[pl.ds(pl.multiple_of(16 + b * tok, 16), tok), lo:hi] = made.astype(bf16)
        for k in range(n_step):

            @pl.when(j == min(n_tp - 1, ((k + 1) * n_tp - 1) // n_step))
            def _():
                w_step(1, k)

        return 0

    lax.fori_loop(0, n_tp, up_block, 0)
    w_own(2)
    for k in range(n_step, n - 1):
        w_step(1, k)
    w_local(1).wait()
    m_drain()

    def gate_block(j, _):
        b = block_of(j)
        for lo in range(0, hid, TILE):
            hi = min(lo + TILE, hid)
            made = lax.dot_general(
                tokens[rows(b), :], gate_full[lo:hi, :], NT, preferred_element_type=f32
            )
            gated = made.astype(bf16).astype(f32)
            window = up_part[pl.ds(pl.multiple_of(b * tok, 16), tok + 16), lo:hi].astype(f32)
            smoothed = bias[:, lo:hi]
            for k in range(3):
                moved = window if k == 2 else pltpu.roll(window, 2 - k, 0)
                smoothed = smoothed + taps[k : k + 1, lo:hi] * moved[16:, :]
            hidden[rows(b), lo:hi] = (jax.nn.gelu(smoothed) * gated).astype(bf16)
        for k in range(min(n_tp - 1, n_step)):

            @pl.when(j == k + 1)
            def _():
                w_step(2, k)

        return 0

    lax.fori_loop(0, n_tp, gate_block, 0)
    w_local(2).wait()

    def shard_of(q):
        d = lax.div(q + 1, 2)
        return ring(jnp.where(lax.rem(q, 2) == 1, -d, d))

    def down_step(q, _):
        for d in range(1, half_n + 1):
            late = [k for k in (2 * d - 2, 2 * d - 1) if min(n_tp - 1, n_step) <= k <= n - 2]
            if late:

                @pl.when(q == 2 * d - 1)
                def _():
                    for k in late:
                        w_step(2, k)

        @pl.when(q < n)
        def _():
            weight = down_full[:, columns(shard_of(q))]
            for dx in range(nx):
                b = x_at(dx) + 1 - 2 * core
                made = jnp.dot(hidden[rows(b), :], weight, preferred_element_type=f32)
                gone(dx, q)[...] = made.astype(bf16)
            for dx in range(nx):
                made = jnp.dot(hidden[rows(x_at(dx)), :], weight, preferred_element_type=f32)
                keep[dx, q] = made.astype(bf16)
                pc_copy(dx, q).start()

        @pl.when((q > 0) & (q < n + 1))
        def _():
            p = q - 1
            for dx in list(range(1, nx)) + [0]:
                pc_copy(dx, p).wait_recv()
                if dx:
                    both = keep[dx, p].astype(f32) + got_core[dx, p].astype(f32)
                    keep[dx, p] = both.astype(bf16)
                    px_copy(dx, p).start()

        @pl.when(q > 1)
        def _():
            p = q - 2
            f = shard_of(p)
            total = stream[:, columns(f)].astype(f32)
            total = total + keep[0, p].astype(f32) + got_core[0, p].astype(f32)
            for dx in range(1, nx):
                px_copy(dx, p).wait_recv()
                total = total + got_x[dx - 1, p].astype(f32)
            held[:, columns(f)] = total.astype(bf16)
            out_copy(f, p).start()

        return 0

    lax.fori_loop(0, n + 2, down_step, 0)

    def finish(q, _):
        out_copy(shard_of(q), q).wait()
        for dx in range(nx):
            pc_copy(dx, q).wait_send()
            if dx:
                px_copy(dx, q).wait_send()
        return 0

    lax.fori_loop(0, n, finish, 0)
    for dx in range(1, nx):
        t_copy(tp, tx_send.at[dx - 1], x_at(dx)).wait_send()
    for dx in range(nx):
        t_copy(x_at(dx), tc_send.at[dx], twin).wait_send()
    for m in range(3):
        w_drain(m)


def make_body(n_fs, n_tp, ny):
    nz, nx = n_fs // ny, n_tp // 2

    def body(
        mixed,
        residual,
        mix_weight,
        norm_gain,
        up_weight,
        gate_weight,
        conv_weight,
        conv_bias,
        down_weight,
    ):
        tok, width = residual.shape
        depth, (hid, wide) = mixed.shape[1], down_weight.shape
        dma = pltpu.SemaphoreType.DMA
        whole = pl.BlockSpec(memory_space=pl.ANY)
        small = pl.BlockSpec(memory_space=pltpu.VMEM)
        return pl.pallas_call(
            functools.partial(layer_kernel, nz, ny, nx),
            out_shape=jax.ShapeDtypeStruct((tok, width), bf16),
            in_specs=[whole] * 6 + [small] * 3,
            out_specs=whole,
            scratch_shapes=[
                pltpu.VMEM((depth, width), bf16),
                pltpu.VMEM((hid, width), bf16),
                pltpu.VMEM((hid, width), bf16),
                pltpu.VMEM((hid, width), bf16),
                pltpu.VMEM((n_tp * tok, width), bf16),
                pltpu.VMEM((n_tp * tok + 16, hid), bf16),
                pltpu.VMEM((n_tp * tok, hid), bf16),
                pltpu.VMEM((tok, depth), bf16),
                pltpu.VMEM((tok, width), bf16),
                pltpu.VMEM((tok, width), bf16),
                pltpu.VMEM((nx, n_fs, tok, wide), bf16),
                pltpu.VMEM((nx, n_fs, tok, wide), bf16),
                pltpu.VMEM((max(nx - 1, 1), n_fs, tok, wide), bf16),
                dma((3, 2, n_fs, 2)),
                dma((3, n_fs, 2)),
                dma((2, n_fs)),
                dma((n_fs, n_tp)),
                dma((n_fs, max(nx - 1, 1))),
                dma((n_fs, nx)),
                dma((n_tp,)),
                dma((max(nx - 1, 1),)),
                dma((nx,)),
                dma((n_fs, nx)),
                dma((n_fs, nx)),
                dma((n_fs, max(nx - 1, 1))),
                dma((n_fs, max(nx - 1, 1))),
                dma((6,)),
                dma((n_fs,)),
            ],
            compiler_params=pltpu.CompilerParams(
                collective_id=0, has_side_effects=True, vmem_limit_bytes=67043328
            ),
        )(
            mixed,
            residual,
            mix_weight,
            up_weight.T,
            gate_weight.T,
            down_weight,
            norm_gain[None, :],
            conv_weight,
            conv_bias[None, :],
        )

    return body


def solution(mesh):
    coords = [getattr(d, "coords", None) for d in mesh.devices[:, 0]]
    n_fs, n_tp = mesh.shape["fs"], mesh.shape["tp"]
    ny = len({c[1] for c in coords}) if None not in coords else 1
    if n_fs % ny:
        ny = 1
    return jax.shard_map(
        make_body(n_fs, n_tp, ny),
        mesh=mesh,
        in_specs=(
            P(("fs", "tp"), None),
            P(("fs", "tp"), None),
            P(("fs", "tp"), None),
            P(),
            P("fs", "tp"),
            P("fs", "tp"),
            P(None, "tp"),
            P("tp"),
            P("tp", "fs"),
        ),
        out_specs=P(("fs", "tp"), None),
        check_vma=False,
    )
```

profile of v0, /device:TPU:0, one launch (start us, length us, event | category | flops | bytes accessed | tf_op | source)
XLA Modules:
  0.0 209.4 jit_solution(16637080693933046989)
XLA Ops:
  0.0 1.3 broadcast_in_dim.7.bias
  1.3 205.3 %shard_map.91 = bf16[384,2048]{1,0:T(8,128)(2,1)} custom-call(bf16[384,2048]{1,0:T(8,128)(2,1)} %mixed.1, bf16[384,2048]{1,0:T(8,128)(2,1)} %residual.1, bf16[64,2048]{1,0:T(8,128)(2,1)} %mix_shard.1, bf16[1376,256]{1,0:T(8,128)(2,1)} %bitcast.3, bf16[1376,256]{1,0:T(8,128)(2,1)} %bitcast.4, bf16[1376,256]{1,0:T(8,128)(2,1)} %down_shard.1, ...), custom_call_target="tpu_custom_call" | custom-call | tf_op jit(solution)/shard_map/pallas_call | solution.py:453
  206.6 2.7 %copy.11 = bf16[384,2048]{1,0:T(8,128)(2,1)} copy(bf16[384,2048]{1,0:T(8,128)(2,1)} %shard_map.91) | data formatting | bytes 3145728
where the time goes:
time: 210 us; the launch traced here: 209 us
  Pallas kernels  205 us (98%)
  local copies, waits for them, and re-layouts  4.02 us (2%)
    pallas_call x1, Pallas kernels, body(): pl.pallas_call(functools.partial(layer_kernel, nz, ny, nx), out_shape=jax...  205 us

commit v1 on v0

--- a/solution.py
+++ b/solution.py
@@ -12,6 +12,7 @@
 MESH = pl.DeviceIdType.MESH
 NT = (((1,), (1,)), ((), ()))
 TILE = 256
+VMEM = 67043328
 
 
 def mod(a, n):
@@ -38,6 +39,7 @@
     nz,
     ny,
     nx,
+    split,
     mixed,
     residual,
     mix_shard,
@@ -55,6 +57,7 @@
     tokens,
     up_part,
     hidden,
+    gate_sum,
     mixed_v,
     held,
     stream,
@@ -65,6 +68,7 @@
     w_recv,
     mr_send,
     m_recv,
+    end_recv,
     mx_send,
     mc_send,
     t_recv,
@@ -85,8 +89,10 @@
     x, core = lax.div(tp, 2), lax.rem(tp, 2)
     place = ring_place(me, nz, ny)
 
+    chips = [ring_chip(mod(place + d, n), nz, ny) for d in range(n)]
+
     def ring(d):
-        return ring_chip(mod(place + d, n), nz, ny)
+        return chips[d % n]
 
     nxt, prv = ring(1), ring(-1)
     twin = tp + 1 - 2 * core
@@ -151,10 +157,14 @@
     def part(f, t):
         return mix_full.at[pl.ds(pl.multiple_of((f * n_tp + t) * mrows, 16), mrows), :]
 
-    def m_ring(f, way, mine=False):
-        src = mix_shard if mine else part(f, tp)
-        to = prv if way else nxt
-        return remote(src, part(f, tp), mr_send.at[way, f], m_recv.at[f, tp], "fs", to)
+    def m_ring(f, way, mine=False, last=False):
+        src, dst = mix_shard if mine else part(f, tp), part(f, tp)
+        to, got = prv if way else nxt, m_recv.at[f, tp]
+        if last:
+            cols = pl.ds(way * (width // 2), width // 2)
+            src = dst = dst.at[:, cols]
+            got = end_recv.at[way]
+        return remote(src, dst, mr_send.at[way, f], got, "fs", to)
 
     def m_x(f, dx, mine=False):
         src = mix_shard if mine else part(f, tp)
@@ -174,13 +184,16 @@
         remote(part(f, t), part(f, t), mc_send.at[f, 0], m_recv.at[f, t], "tp", twin).wait_recv()
 
     def m_step(d):
+        if d == half_n:
+            for way in range(2):
+                m_ring(ring(d), way, last=True).wait_recv()
+            m_spread(ring(d))
+            return
         for way in range(2):
-            if d < half_n + 1 - way:
-                f = ring(d if way else -d)
-                m_wait(f, tp)
-                if d < half_n - way:
-                    m_ring(f, way).start()
-                m_spread(f)
+            f = ring(d if way else -d)
+            m_wait(f, tp)
+            m_ring(f, way, last=d == half_n - 1).start()
+            m_spread(f)
 
     def m_relay(f):
         for dx in range(1, nx):
@@ -193,8 +206,8 @@
             f = ring(-d if q % 2 else d)
             mine = q == 0
             for way in range(2):
-                if d < half_n - way and (mine or (q % 2 == 1) == (way == 0)):
-                    m_ring(f, way, mine).wait_send()
+                if d < half_n and (mine or (q % 2 == 1) == (way == 0)):
+                    m_ring(f, way, mine, d == half_n - 1).wait_send()
             for dx in range(1, nx):
                 m_x(f, dx, mine).wait_send()
             for dx in range(nx):
@@ -250,7 +263,6 @@
     load_mix.start()
     load_mixed.start()
     load_residual.start()
-    w_own(0)
     for m in range(3):
         w_local(m).start()
     up_part[0:16, :] = jnp.zeros((16, hid), bf16)
@@ -258,6 +270,8 @@
     early = min(n_step, half_n - 1)
     for d in range(1, half_n + 1):
         m_step(d)
+        if d == 1:
+            w_own(0)
         if 2 <= d < early + 2:
             w_step(0, d - 2)
     for q in range(n):
@@ -322,86 +336,118 @@
                 tokens[rows(b), :], up_full[lo:hi, :], NT, preferred_element_type=f32
             )
             up_part[pl.ds(pl.multiple_of(16 + b * tok, 16), tok), lo:hi] = made.astype(bf16)
-        for k in range(n_step):
-
-            @pl.when(j == min(n_tp - 1, ((k + 1) * n_tp - 1) // n_step))
-            def _():
+        for at, ks in ((1, (0, 1)), (n_tp - 2, (2,))):
+            for k in ks:
+                if k < ahead:
+
+                    @pl.when(j == at)
+                    def _():
+                        w_step(1, k)
+
+        return 0
+
+    ahead = min(3, n_step)
+    lax.fori_loop(0, n_tp, up_block, 0)
+
+    def gate_dot(b, lo, hi, fs):
+        made = None
+        for f in fs:
+            term = lax.dot_general(
+                tokens[rows(b), columns(f)],
+                gate_full[lo:hi, columns(f)],
+                NT,
+                preferred_element_type=f32,
+            )
+            made = term if made is None else made + term
+        return made
+
+    def gate_pass(d):
+        fs = ([me] if d == 1 else []) + [ring(-d), ring(d)]
+
+        def add(b, _):
+            for lo in range(0, hid, TILE):
+                hi = min(lo + TILE, hid)
+                made = gate_dot(b, lo, hi, fs)
+                if d > 1:
+                    made = gate_sum[rows(b), lo:hi] + made
+                gate_sum[rows(b), lo:hi] = made
+            return 0
+
+        lax.fori_loop(0, n_tp, add, 0)
+
+    w_local(1).wait()
+    for d in range(1, half_n):
+        for k in (2 * d - 2, 2 * d - 1):
+            if k >= ahead:
                 w_step(1, k)
-
-        return 0
-
-    lax.fori_loop(0, n_tp, up_block, 0)
-    w_own(2)
-    for k in range(n_step, n - 1):
-        w_step(1, k)
-    w_local(1).wait()
+            if k == n_step - 1:
+                w_own(2)
+        if split:
+            gate_pass(d)
+    w_step(1, n - 2)
     m_drain()
 
     def gate_block(j, _):
         b = block_of(j)
         for lo in range(0, hid, TILE):
             hi = min(lo + TILE, hid)
-            made = lax.dot_general(
-                tokens[rows(b), :], gate_full[lo:hi, :], NT, preferred_element_type=f32
-            )
+            if split:
+                made = gate_sum[rows(b), lo:hi] + gate_dot(b, lo, hi, [ring(half_n)])
+            else:
+                made = lax.dot_general(
+                    tokens[rows(b), :], gate_full[lo:hi, :], NT, preferred_element_type=f32
+                )
             gated = made.astype(bf16).astype(f32)
             window = up_part[pl.ds(pl.multiple_of(b * tok, 16), tok + 16), lo:hi].astype(f32)
-            smoothed = bias[:, lo:hi]
+            smoothed = bias[lo:hi][None, :]
             for k in range(3):
                 moved = window if k == 2 else pltpu.roll(window, 2 - k, 0)
                 smoothed = smoothed + taps[k : k + 1, lo:hi] * moved[16:, :]
             hidden[rows(b), lo:hi] = (jax.nn.gelu(smoothed) * gated).astype(bf16)
-        for k in range(min(n_tp - 1, n_step)):
-
-            @pl.when(j == k + 1)
+
+        @pl.when(j == n_tp - 2)
+        def _():
+            w_step(2, 0)
+
+        return 0
+
+    lax.fori_loop(0, n_tp, gate_block, 0)
+    w_local(2).wait()
+
+    def shard_of(q):
+        d = lax.div(q + 1, 2)
+        return ring_chip(mod(place + jnp.where(lax.rem(q, 2) == 1, -d, d), n), nz, ny)
+
+    others = list(range(1, nx)) + [0]
+
+    def down_step(q, _):
+        for k in range(1, n - 1):
+
+            @pl.when(q == (k if k < n - 2 else n - 1))
             def _():
                 w_step(2, k)
-
-        return 0
-
-    lax.fori_loop(0, n_tp, gate_block, 0)
-    w_local(2).wait()
-
-    def shard_of(q):
-        d = lax.div(q + 1, 2)
-        return ring(jnp.where(lax.rem(q, 2) == 1, -d, d))
-
-    def down_step(q, _):
-        for d in range(1, half_n + 1):
-            late = [k for k in (2 * d - 2, 2 * d - 1) if min(n_tp - 1, n_step) <= k <= n - 2]
-            if late:
-
-                @pl.when(q == 2 * d - 1)
-                def _():
-                    for k in late:
-                        w_step(2, k)
 
         @pl.when(q < n)
         def _():
             weight = down_full[:, columns(shard_of(q))]
-            for dx in range(nx):
+            for dx in others:
                 b = x_at(dx) + 1 - 2 * core
                 made = jnp.dot(hidden[rows(b), :], weight, preferred_element_type=f32)
                 gone(dx, q)[...] = made.astype(bf16)
-            for dx in range(nx):
                 made = jnp.dot(hidden[rows(x_at(dx)), :], weight, preferred_element_type=f32)
                 keep[dx, q] = made.astype(bf16)
                 pc_copy(dx, q).start()
-
-        @pl.when((q > 0) & (q < n + 1))
-        def _():
-            p = q - 1
-            for dx in list(range(1, nx)) + [0]:
-                pc_copy(dx, p).wait_recv()
-                if dx:
-                    both = keep[dx, p].astype(f32) + got_core[dx, p].astype(f32)
-                    keep[dx, p] = both.astype(bf16)
-                    px_copy(dx, p).start()
+            for dx in range(1, nx):
+                pc_copy(dx, q).wait_recv()
+                both = keep[dx, q].astype(f32) + got_core[dx, q].astype(f32)
+                keep[dx, q] = both.astype(bf16)
+                px_copy(dx, q).start()
 
         @pl.when(q > 1)
         def _():
             p = q - 2
             f = shard_of(p)
+            pc_copy(0, p).wait_recv()
             total = stream[:, columns(f)].astype(f32)
             total = total + keep[0, p].astype(f32) + got_core[0, p].astype(f32)
             for dx in range(1, nx):
@@ -450,8 +496,12 @@
         dma = pltpu.SemaphoreType.DMA
         whole = pl.BlockSpec(memory_space=pl.ANY)
         small = pl.BlockSpec(memory_space=pltpu.VMEM)
+        held = depth + 3 * hid + n_tp * tok + (3 * nx + 2) * tok
+        lanes = (hid + 127) // 128 * 128
+        held = held * width * 2 + n_tp * tok * lanes * 8 + (1 << 20)
+        split = held <= VMEM
         return pl.pallas_call(
-            functools.partial(layer_kernel, nz, ny, nx),
+            functools.partial(layer_kernel, nz, ny, nx, split),
             out_shape=jax.ShapeDtypeStruct((tok, width), bf16),
             in_specs=[whole] * 6 + [small] * 3,
             out_specs=whole,
@@ -463,6 +513,7 @@
                 pltpu.VMEM((n_tp * tok, width), bf16),
                 pltpu.VMEM((n_tp * tok + 16, hid), bf16),
                 pltpu.VMEM((n_tp * tok, hid), bf16),
+                pltpu.VMEM((n_tp * tok, hid) if split else (8, 128), f32),
                 pltpu.VMEM((tok, depth), bf16),
                 pltpu.VMEM((tok, width), bf16),
                 pltpu.VMEM((tok, width), bf16),
@@ -473,6 +524,7 @@
                 dma((3, n_fs, 2)),
                 dma((2, n_fs)),
                 dma((n_fs, n_tp)),
+                dma((2,)),
                 dma((n_fs, max(nx - 1, 1))),
                 dma((n_fs, nx)),
                 dma((n_tp,)),
@@ -486,7 +538,7 @@
                 dma((n_fs,)),
             ],
             compiler_params=pltpu.CompilerParams(
-                collective_id=0, has_side_effects=True, vmem_limit_bytes=67043328
+                collective_id=0, has_side_effects=True, vmem_limit_bytes=VMEM
             ),
         )(
             mixed,
@@ -497,7 +549,7 @@
             down_weight,
             norm_gain[None, :],
             conv_weight,
-            conv_bias[None, :],
+            conv_bias,
         )
 
     return body

time: 210 us -> 201 us (0.957)
  Pallas kernels: 205 us -> 199 us
    pallas_call x1, Pallas kernels: 205 us -> 199 us  [body(): pl.pallas_call(functools.partial(layer_kernel, nz, ny, nx, split), out_sh...]
where the time goes in v1:
time: 201 us
  Pallas kernels  199 us (99%)
  local copies, waits for them, and re-layouts  2.73 us (1%)
    pallas_call x1, Pallas kernels, body(): pl.pallas_call(functools.partial(layer_kernel, nz, ny, nx, split), out_sh...  199 us

profile of v1, /device:TPU:0, one launch (start us, length us, event | category | flops | bytes accessed | tf_op | source)
XLA Modules:
  0.0 201.3 jit_solution(14989065187559310443)
XLA Ops:
  0.0 198.5 %shard_map.91 = bf16[384,2048]{1,0:T(8,128)(2,1)} custom-call(bf16[384,2048]{1,0:T(8,128)(2,1)} %mixed.1, bf16[384,2048]{1,0:T(8,128)(2,1)} %residual.1, bf16[64,2048]{1,0:T(8,128)(2,1)} %mix_shard.1, bf16[1376,256]{1,0:T(8,128)(2,1)} %bitcast.3, bf16[1376,256]{1,0:T(8,128)(2,1)} %bitcast.4, bf16[1376,256]{1,0:T(8,128)(2,1)} %down_shard.1, ...), custom_call_target="tpu_custom_call" | custom-call | tf_op jit(solution)/shard_map/pallas_call | solution.py:503
  198.5 2.7 %copy.11 = bf16[384,2048]{1,0:T(8,128)(2,1)} copy(bf16[384,2048]{1,0:T(8,128)(2,1)} %shard_map.91) | data formatting | bytes 3145728

commit v2 on v1

--- a/solution.py
+++ b/solution.py
@@ -49,7 +49,7 @@
     gain,
     taps,
     bias,
-    out,
+    held,
     mix_full,
     up_full,
     gate_full,
@@ -59,27 +59,21 @@
     hidden,
     gate_sum,
     mixed_v,
-    held,
     stream,
     keep,
     got_core,
     got_x,
     w_send,
     w_recv,
-    mr_send,
+    m_send,
     m_recv,
     end_recv,
-    mx_send,
-    mc_send,
+    t_send,
     t_recv,
-    tx_send,
-    tc_send,
-    pc_send,
+    p_send,
     pc_recv,
-    px_send,
     px_recv,
     in_sem,
-    out_sem,
 ):
     n = nz * ny
     half_n = n // 2
@@ -102,8 +96,9 @@
 
     tok, width = stream.shape
     hid, wide = up_shard.shape
-    cut = (hid // 2 + 15) // 16 * 16
-    halves = ((0, cut), (cut, hid - cut))
+    by_columns = wide % 256 == 0
+    cut = wide // 2 if by_columns else (hid // 2 + 15) // 16 * 16
+    halves = ((0, cut), (cut, (wide if by_columns else hid) - cut))
     fulls = (up_full, gate_full, down_full)
     shards = (up_shard, gate_shard, down_shard)
     n_step = n - 3
@@ -119,15 +114,22 @@
             device_id_type=MESH,
         )
 
+    def columns(f):
+        return pl.ds(pl.multiple_of(f * wide, 128), wide)
+
     def slot(m, f, h):
         off, size = halves[h]
-        return fulls[m].at[pl.ds(off, size), pl.ds(pl.multiple_of(f * wide, 128), wide)]
+        if by_columns:
+            return fulls[m].at[:, pl.ds(pl.multiple_of(f * wide + off, 128), size)]
+        return fulls[m].at[pl.ds(off, size), columns(f)]
 
     def w_copy(m, f, h, way, mine=False):
-        off, size = halves[h]
-        src = shards[m].at[pl.ds(off, size), :] if mine else slot(m, f, h)
+        at = pl.ds(*halves[h])
+        src = slot(m, f, h)
+        if mine:
+            src = shards[m].at[:, at] if by_columns else shards[m].at[at, :]
         to = prv if way else nxt
-        return remote(src, slot(m, f, h), w_send.at[m, way, f, h], w_recv.at[m, f, h], "fs", to)
+        return remote(src, slot(m, f, h), w_send.at[m], w_recv.at[m, f, h], "fs", to)
 
     def w_own(m):
         for k in range(2):
@@ -141,47 +143,43 @@
             if k < n_step:
                 w_copy(m, f, hh, way).start()
 
+    def sent(ref, sem):
+        remote(ref, ref, sem, sem, "fs", nxt).wait_send()
+
     def w_drain(m):
-        for h in range(2):
-            for way in range(2):
-                w_copy(m, me, h, way, True).wait_send()
-        for k in range(n_step):
-            d, h = 1 + k // 2, k % 2
-            w_copy(m, ring(-d), h, 0).wait_send()
-            w_copy(m, ring(d), 1 - h, 1).wait_send()
+        sent(fulls[m].at[:, pl.ds(0, (n - 1) * wide)], w_send.at[m])
 
     def w_local(m):
-        cols = pl.ds(pl.multiple_of(me * wide, 128), wide)
-        return pltpu.make_async_copy(shards[m], fulls[m].at[:, cols], in_sem.at[m])
+        return pltpu.make_async_copy(shards[m], fulls[m].at[:, columns(me)], in_sem.at[m])
 
     def part(f, t):
         return mix_full.at[pl.ds(pl.multiple_of((f * n_tp + t) * mrows, 16), mrows), :]
 
     def m_ring(f, way, mine=False, last=False):
         src, dst = mix_shard if mine else part(f, tp), part(f, tp)
-        to, got = prv if way else nxt, m_recv.at[f, tp]
+        to, got = prv if way else nxt, m_recv.at[f, 0]
         if last:
             cols = pl.ds(way * (width // 2), width // 2)
             src = dst = dst.at[:, cols]
             got = end_recv.at[way]
-        return remote(src, dst, mr_send.at[way, f], got, "fs", to)
+        return remote(src, dst, m_send.at[0], got, "fs", to)
 
     def m_x(f, dx, mine=False):
         src = mix_shard if mine else part(f, tp)
-        return remote(src, part(f, tp), mx_send.at[f, dx - 1], m_recv.at[f, tp], "tp", x_at(dx))
+        return remote(src, part(f, tp), m_send.at[1], m_recv.at[f, dx], "tp", x_at(dx))
 
     def m_core(f, dx, mine=False):
         t = x_at(dx)
         src = mix_shard if mine else part(f, t)
-        return remote(src, part(f, t), mc_send.at[f, dx], m_recv.at[f, t], "tp", twin)
+        return remote(src, part(f, t), m_send.at[2], end_recv.at[2], "tp", twin)
 
     def m_spread(f, mine=False):
         for dx in range(1, nx):
             m_x(f, dx, mine).start()
         m_core(f, 0, mine).start()
 
-    def m_wait(f, t):
-        remote(part(f, t), part(f, t), mc_send.at[f, 0], m_recv.at[f, t], "tp", twin).wait_recv()
+    def m_wait(f, t, got):
+        remote(part(f, t), part(f, t), m_send.at[2], got, "tp", twin).wait_recv()
 
     def m_step(d):
         if d == half_n:
@@ -191,27 +189,18 @@
             return
         for way in range(2):
             f = ring(d if way else -d)
-            m_wait(f, tp)
+            m_wait(f, tp, m_recv.at[f, 0])
             m_ring(f, way, last=d == half_n - 1).start()
             m_spread(f)
 
     def m_relay(f):
         for dx in range(1, nx):
-            m_wait(f, x_at(dx))
+            m_wait(f, x_at(dx), m_recv.at[f, nx - dx])
             m_core(f, dx).start()
 
     def m_drain():
-        for q in range(n):
-            d = (q + 1) // 2
-            f = ring(-d if q % 2 else d)
-            mine = q == 0
-            for way in range(2):
-                if d < half_n and (mine or (q % 2 == 1) == (way == 0)):
-                    m_ring(f, way, mine, d == half_n - 1).wait_send()
-            for dx in range(1, nx):
-                m_x(f, dx, mine).wait_send()
-            for dx in range(nx):
-                m_core(f, dx, mine and dx == 0).wait_send()
+        for lane, count in enumerate((n - 1, n * (nx - 1), n * nx)):
+            sent(mix_full.at[pl.ds(0, count * mrows), :], m_send.at[lane])
 
     def rows(b):
         return pl.ds(pl.multiple_of(b * tok, 16), tok)
@@ -220,31 +209,25 @@
         return remote(tokens.at[rows(b), :], tokens.at[rows(b), :], send, t_recv.at[b], "tp", to)
 
     def t_wait(b):
-        t_copy(b, tc_send.at[0], twin).wait_recv()
-
-    def columns(f):
-        return pl.ds(pl.multiple_of(f * wide, 128), wide)
+        t_copy(b, t_send.at[1], twin).wait_recv()
 
     def gone(dx, q):
         return mix_full.at[pl.ds(dx * tok, tok), columns(q)]
 
     def pc_copy(dx, q):
         return remote(
-            gone(dx, q), got_core.at[dx, q], pc_send.at[q, dx], pc_recv.at[q, dx], "tp", twin
+            gone(dx, q), got_core.at[dx, q], p_send.at[0], pc_recv.at[q, dx], "tp", twin
         )
 
     def px_copy(dx, q):
         return remote(
             keep.at[dx, q],
             got_x.at[dx - 1, q],
-            px_send.at[q, dx - 1],
+            p_send.at[1],
             px_recv.at[q, dx - 1],
             "tp",
             x_at(dx),
         )
-
-    def out_copy(f, q):
-        return pltpu.make_async_copy(held.at[:, columns(f)], out.at[:, columns(f)], out_sem.at[q])
 
     load_mixed = pltpu.make_async_copy(mixed, mixed_v, in_sem.at[3])
     load_residual = pltpu.make_async_copy(residual, held, in_sem.at[4])
@@ -277,9 +260,8 @@
     for q in range(n):
         d = (q + 1) // 2
         m_relay(ring(-d if q % 2 else d))
-    for f in range(n):
-        for dx in range(nx):
-            m_wait(f, x_at(dx) + 1 - 2 * core)
+    from_twin = mix_full.at[pl.ds(0, n * nx * mrows), :]
+    remote(from_twin, from_twin, m_send.at[2], end_recv.at[2], "tp", twin).wait_recv()
     load_mix.wait()
     load_mixed.wait()
     load_residual.wait()
@@ -306,8 +288,8 @@
 
     lax.fori_loop(0, tok // 32, norm, 0)
     for dx in range(1, nx):
-        t_copy(tp, tx_send.at[dx - 1], x_at(dx)).start()
-    t_copy(tp, tc_send.at[0], twin).start()
+        t_copy(tp, t_send.at[0], x_at(dx)).start()
+    t_copy(tp, t_send.at[1], twin).start()
 
     for k in range(min(early + 1, n_step), n_step):
         w_step(0, k)
@@ -328,7 +310,7 @@
 
         @pl.when((j > 1) & (lax.rem(j, 2) == 0))
         def _():
-            t_copy(b, tc_send.at[lax.div(j, 2)], twin).start()
+            t_copy(b, t_send.at[1], twin).start()
 
         for lo in range(0, hid, TILE):
             hi = min(lo + TILE, hid)
@@ -386,6 +368,10 @@
             gate_pass(d)
     w_step(1, n - 2)
     m_drain()
+    for lane in range(2):
+        sent(tokens.at[pl.ds(0, (nx - 1 + lane) * tok), :], t_send.at[lane])
+    for m in range(2):
+        w_drain(m)
 
     def gate_block(j, _):
         b = block_of(j)
@@ -414,22 +400,32 @@
     lax.fori_loop(0, n_tp, gate_block, 0)
     w_local(2).wait()
 
-    def shard_of(q):
-        d = lax.div(q + 1, 2)
-        return ring_chip(mod(place + jnp.where(lax.rem(q, 2) == 1, -d, d), n), nz, ny)
+    def pieces(q):
+        if not by_columns:
+            d = lax.div(q + 1, 2)
+            d = jnp.where(lax.rem(q, 2) == 1, -d, d)
+            return [columns(ring_chip(mod(place + d, n), nz, ny))]
+        k = jnp.maximum(q - 1, 0)
+        d, h = jnp.where(q == 0, 0, 1 + lax.div(k, 2)), lax.rem(k, 2)
+        left = ring_chip(mod(place - d, n), nz, ny) * wide + h * cut
+        right = ring_chip(mod(place + d, n), nz, ny) * wide + (1 - h) * cut
+        return [pl.ds(pl.multiple_of(at, 128), cut) for at in (left, right)]
+
+    def step_at(k):
+        return k + 1 if by_columns else k if k < n - 2 else n - 1
 
     others = list(range(1, nx)) + [0]
 
     def down_step(q, _):
         for k in range(1, n - 1):
 
-            @pl.when(q == (k if k < n - 2 else n - 1))
+            @pl.when(q == step_at(k))
             def _():
                 w_step(2, k)
 
         @pl.when(q < n)
         def _():
-            weight = down_full[:, columns(shard_of(q))]
+            weight = jnp.concatenate([down_full[:, cols] for cols in pieces(q)], axis=1)
             for dx in others:
                 b = x_at(dx) + 1 - 2 * core
                 made = jnp.dot(hidden[rows(b), :], weight, preferred_element_type=f32)
@@ -446,35 +442,25 @@
         @pl.when(q > 1)
         def _():
             p = q - 2
-            f = shard_of(p)
             pc_copy(0, p).wait_recv()
-            total = stream[:, columns(f)].astype(f32)
-            total = total + keep[0, p].astype(f32) + got_core[0, p].astype(f32)
+            total = keep[0, p].astype(f32) + got_core[0, p].astype(f32)
             for dx in range(1, nx):
                 px_copy(dx, p).wait_recv()
                 total = total + got_x[dx - 1, p].astype(f32)
-            held[:, columns(f)] = total.astype(bf16)
-            out_copy(f, p).start()
+            off = 0
+            for cols in pieces(p):
+                size = cols.size
+                whole = stream[:, cols].astype(f32) + total[:, off : off + size]
+                held[:, cols] = whole.astype(bf16)
+                off += size
 
         return 0
 
     lax.fori_loop(0, n + 2, down_step, 0)
-
-    def finish(q, _):
-        out_copy(shard_of(q), q).wait()
-        for dx in range(nx):
-            pc_copy(dx, q).wait_send()
-            if dx:
-                px_copy(dx, q).wait_send()
-        return 0
-
-    lax.fori_loop(0, n, finish, 0)
+    sent(mix_full.at[pl.ds(0, nx * tok), :], p_send.at[0])
     for dx in range(1, nx):
-        t_copy(tp, tx_send.at[dx - 1], x_at(dx)).wait_send()
-    for dx in range(nx):
-        t_copy(x_at(dx), tc_send.at[dx], twin).wait_send()
-    for m in range(3):
-        w_drain(m)
+        sent(mix_full.at[pl.ds(0, tok), :], p_send.at[1])
+    w_drain(2)
 
 
 def make_body(n_fs, n_tp, ny):
@@ -502,9 +488,9 @@
         split = held <= VMEM
         return pl.pallas_call(
             functools.partial(layer_kernel, nz, ny, nx, split),
-            out_shape=jax.ShapeDtypeStruct((tok, width), bf16),
+            out_shape=pltpu.VMEM((tok, width), bf16),
             in_specs=[whole] * 6 + [small] * 3,
-            out_specs=whole,
+            out_specs=small,
             scratch_shapes=[
                 pltpu.VMEM((depth, width), bf16),
                 pltpu.VMEM((hid, width), bf16),
@@ -516,29 +502,23 @@
                 pltpu.VMEM((n_tp * tok, hid) if split else (8, 128), f32),
                 pltpu.VMEM((tok, depth), bf16),
                 pltpu.VMEM((tok, width), bf16),
-                pltpu.VMEM((tok, width), bf16),
                 pltpu.VMEM((nx, n_fs, tok, wide), bf16),
                 pltpu.VMEM((nx, n_fs, tok, wide), bf16),
                 pltpu.VMEM((max(nx - 1, 1), n_fs, tok, wide), bf16),
-                dma((3, 2, n_fs, 2)),
+                dma((3,)),
                 dma((3, n_fs, 2)),
-                dma((2, n_fs)),
-                dma((n_fs, n_tp)),
+                dma((3,)),
+                dma((n_fs, nx)),
+                dma((3,)),
                 dma((2,)),
-                dma((n_fs, max(nx - 1, 1))),
-                dma((n_fs, nx)),
                 dma((n_tp,)),
-                dma((max(nx - 1, 1),)),
-                dma((nx,)),
-                dma((n_fs, nx)),
+                dma((2,)),
                 dma((n_fs, nx)),
                 dma((n_fs, max(nx - 1, 1))),
-                dma((n_fs, max(nx - 1, 1))),
                 dma((6,)),
-                dma((n_fs,)),
             ],
             compiler_params=pltpu.CompilerParams(
-                collective_id=0, has_side_effects=True, vmem_limit_bytes=VMEM
+                collective_id=0, has_side_effects=True, vmem_limit_bytes=VMEM - 2 * tok * width * 2
             ),
         )(
             mixed,

time: 201 us -> 197 us (0.980)
  Pallas kernels: 199 us -> 195 us
    pallas_call x1, Pallas kernels: 199 us -> 195 us  [body(): pl.pallas_call(functools.partial(layer_kernel, nz, ny, nx, split), out_sh...]
where the time goes in v2:
time: 197 us
  Pallas kernels  195 us (99%)
    pallas_call x1, Pallas kernels, body(): pl.pallas_call(functools.partial(layer_kernel, nz, ny, nx, split), out_sh...  195 us

profile of v2, /device:TPU:0, one launch (start us, length us, event | category | flops | bytes accessed | tf_op | source)
XLA Modules:
  0.0 196.5 jit_solution(10865443230338111424)
XLA Ops:
  0.0 195.4 %shard_map.91 = bf16[384,2048]{1,0:T(8,128)(2,1)S(1)} custom-call(bf16[384,2048]{1,0:T(8,128)(2,1)} %mixed.1, bf16[384,2048]{1,0:T(8,128)(2,1)} %residual.1, bf16[64,2048]{1,0:T(8,128)(2,1)} %mix_shard.1, bf16[1376,256]{1,0:T(8,128)(2,1)} %bitcast.3, bf16[1376,256]{1,0:T(8,128)(2,1)} %bitcast.4, bf16[1376,256]{1,0:T(8,128)(2,1)} %down_shard.1, ...), custom_call_target="tpu_custom_call" | custom-call | tf_op jit(solution)/shard_map/pallas_call | solution.py:489
  195.4 1.1 copy.11

commit v3 on v2

--- a/solution.py
+++ b/solution.py
@@ -66,8 +66,9 @@
     w_send,
     w_recv,
     m_send,
+    m_ring_recv,
     m_recv,
-    end_recv,
+    m_core_recv,
     t_send,
     t_recv,
     p_send,
@@ -103,6 +104,9 @@
     shards = (up_shard, gate_shard, down_shard)
     n_step = n - 3
     mrows = mix_shard.shape[0]
+    front = width // 2
+    mix_cut = ((0, front), (front, width - front))
+    n_piece, piece = keep.shape[1], keep.shape[3]
 
     def remote(src, dst, send, recv, axis, to):
         return pltpu.make_async_remote_copy(
@@ -136,9 +140,10 @@
             w_copy(m, me, k, 0, True).start()
             w_copy(m, me, 1 - k, 1, True).start()
 
-    def w_step(m, k):
-        d, h = 1 + k // 2, k % 2
-        for way, f, hh in ((0, ring(-d), h), (1, ring(d), 1 - h)):
+    def w_step(m, k, ways=(0, 1)):
+        d = 1 + k // 2
+        for way in ways:
+            f, hh = (ring(d), 1 - k % 2) if way else (ring(-d), k % 2)
             w_copy(m, f, hh, way).wait_recv()
             if k < n_step:
                 w_copy(m, f, hh, way).start()
@@ -155,23 +160,24 @@
     def part(f, t):
         return mix_full.at[pl.ds(pl.multiple_of((f * n_tp + t) * mrows, 16), mrows), :]
 
-    def m_ring(f, way, mine=False, last=False):
-        src, dst = mix_shard if mine else part(f, tp), part(f, tp)
-        to, got = prv if way else nxt, m_recv.at[f, 0]
-        if last:
-            cols = pl.ds(way * (width // 2), width // 2)
-            src = dst = dst.at[:, cols]
-            got = end_recv.at[way]
-        return remote(src, dst, m_send.at[0], got, "fs", to)
+    def m_half(f, h):
+        return part(f, tp).at[:, pl.ds(*mix_cut[h])]
+
+    def m_ring(f, h, way, mine=False):
+        src = m_half(f, h)
+        if mine:
+            src = mix_shard.at[:, pl.ds(*mix_cut[h])]
+        to = prv if way else nxt
+        return remote(src, m_half(f, h), m_send.at[0], m_ring_recv.at[f, h], "fs", to)
 
     def m_x(f, dx, mine=False):
         src = mix_shard if mine else part(f, tp)
-        return remote(src, part(f, tp), m_send.at[1], m_recv.at[f, dx], "tp", x_at(dx))
+        return remote(src, part(f, tp), m_send.at[1], m_recv.at[f, dx - 1], "tp", x_at(dx))
 
     def m_core(f, dx, mine=False):
         t = x_at(dx)
         src = mix_shard if mine else part(f, t)
-        return remote(src, part(f, t), m_send.at[2], end_recv.at[2], "tp", twin)
+        return remote(src, part(f, t), m_send.at[2], m_core_recv.at[0], "tp", twin)
 
     def m_spread(f, mine=False):
         for dx in range(1, nx):
@@ -181,21 +187,24 @@
     def m_wait(f, t, got):
         remote(part(f, t), part(f, t), m_send.at[2], got, "tp", twin).wait_recv()
 
+    def m_own():
+        for k in range(2):
+            m_ring(me, k, 0, True).start()
+            m_ring(me, 1 - k, 1, True).start()
+
     def m_step(d):
-        if d == half_n:
-            for way in range(2):
-                m_ring(ring(d), way, last=True).wait_recv()
-            m_spread(ring(d))
-            return
-        for way in range(2):
-            f = ring(d if way else -d)
-            m_wait(f, tp, m_recv.at[f, 0])
-            m_ring(f, way, last=d == half_n - 1).start()
+        for k in (2 * d - 2, 2 * d - 1):
+            for way, f, h in ((0, ring(-d), k % 2), (1, ring(d), 1 - k % 2)):
+                if k < n - 1:
+                    m_ring(f, h, way).wait_recv()
+                if k < n_step:
+                    m_ring(f, h, way).start()
+        for f in (ring(-d), ring(d)) if d < half_n else (ring(d),):
             m_spread(f)
 
     def m_relay(f):
         for dx in range(1, nx):
-            m_wait(f, x_at(dx), m_recv.at[f, nx - dx])
+            m_wait(f, x_at(dx), m_recv.at[f, nx - dx - 1])
             m_core(f, dx).start()
 
     def m_drain():
@@ -212,7 +221,8 @@
         t_copy(b, t_send.at[1], twin).wait_recv()
 
     def gone(dx, q):
-        return mix_full.at[pl.ds(dx * tok, tok), columns(q)]
+        at = pl.multiple_of(q * piece, 128)
+        return mix_full.at[pl.ds(dx * tok, tok), pl.ds(at, piece)]
 
     def pc_copy(dx, q):
         return remote(
@@ -220,14 +230,8 @@
         )
 
     def px_copy(dx, q):
-        return remote(
-            keep.at[dx, q],
-            got_x.at[dx - 1, q],
-            p_send.at[1],
-            px_recv.at[q, dx - 1],
-            "tp",
-            x_at(dx),
-        )
+        src, dst = keep.at[dx, q], got_x.at[dx - 1, q]
+        return remote(src, dst, p_send.at[1], px_recv.at[q, dx - 1], "tp", x_at(dx))
 
     load_mixed = pltpu.make_async_copy(mixed, mixed_v, in_sem.at[3])
     load_residual = pltpu.make_async_copy(residual, held, in_sem.at[4])
@@ -240,8 +244,7 @@
         pl.semaphore_signal(barrier, inc=1, device_id={"tp": other}, device_id_type=MESH)
     pl.semaphore_wait(barrier, 2 + nx)
 
-    m_ring(me, 0, True).start()
-    m_ring(me, 1, True).start()
+    m_own()
     m_spread(me, True)
     load_mix.start()
     load_mixed.start()
@@ -261,7 +264,7 @@
         d = (q + 1) // 2
         m_relay(ring(-d if q % 2 else d))
     from_twin = mix_full.at[pl.ds(0, n * nx * mrows), :]
-    remote(from_twin, from_twin, m_send.at[2], end_recv.at[2], "tp", twin).wait_recv()
+    remote(from_twin, from_twin, m_send.at[2], m_core_recv.at[0], "tp", twin).wait_recv()
     load_mix.wait()
     load_mixed.wait()
     load_residual.wait()
@@ -400,63 +403,84 @@
     lax.fori_loop(0, n_tp, gate_block, 0)
     w_local(2).wait()
 
-    def pieces(q):
-        if not by_columns:
-            d = lax.div(q + 1, 2)
-            d = jnp.where(lax.rem(q, 2) == 1, -d, d)
-            return [columns(ring_chip(mod(place + d, n), nz, ny))]
-        k = jnp.maximum(q - 1, 0)
-        d, h = jnp.where(q == 0, 0, 1 + lax.div(k, 2)), lax.rem(k, 2)
-        left = ring_chip(mod(place - d, n), nz, ny) * wide + h * cut
-        right = ring_chip(mod(place + d, n), nz, ny) * wide + (1 - h) * cut
-        return [pl.ds(pl.multiple_of(at, 128), cut) for at in (left, right)]
-
-    def step_at(k):
-        return k + 1 if by_columns else k if k < n - 2 else n - 1
-
-    others = list(range(1, nx)) + [0]
+    def piece_columns(q):
+        if by_columns:
+            k, way = lax.div(jnp.maximum(q - 2, 0), 2), lax.rem(q, 2)
+            d = jnp.where(q < 2, 0, 1 + lax.div(k, 2))
+            h = jnp.where(way == 0, lax.rem(k, 2), 1 - lax.rem(k, 2))
+        else:
+            d, h, way = lax.div(q + 1, 2), 0, 1 - lax.rem(q, 2)
+        f = ring_chip(mod(place + jnp.where(way == 0, -d, d), n), nz, ny)
+        return pl.ds(pl.multiple_of(f * wide + h * piece, 128), piece)
+
+    def steps_before(q):
+        if by_columns:
+            k = (q - 2) // 2
+            return [(k, (q % 2,))] if 0 < k else []
+        ks = [n - 2] if q == n - 1 else [q] if 0 < q < n - 2 else []
+        return [(k, (0, 1)) for k in ks]
+
+    def product(q, b):
+        made = jnp.dot(
+            hidden[rows(b), :], down_full[:, piece_columns(q)], preferred_element_type=f32
+        )
+        return made.astype(bf16)
+
+    def make(q, dx):
+        gone(dx, q)[...] = product(q, x_at(dx) + 1 - 2 * core)
+        keep[dx, q] = product(q, x_at(dx))
+        pc_copy(dx, q).start()
+
+    def make_far(q):
+        for dx in range(1, nx):
+            make(q, dx)
+
+    def pair_far(q):
+        for dx in range(1, nx):
+            pc_copy(dx, q).wait_recv()
+            both = keep[dx, q].astype(f32) + got_core[dx, q].astype(f32)
+            keep[dx, q] = both.astype(bf16)
+            px_copy(dx, q).start()
+
+    def finish(q):
+        cols = piece_columns(q)
+        pc_copy(0, q).wait_recv()
+        total = stream[:, cols].astype(f32) + keep[0, q].astype(f32)
+        total = total + got_core[0, q].astype(f32)
+        for dx in range(1, nx):
+            px_copy(dx, q).wait_recv()
+            total = total + got_x[dx - 1, q].astype(f32)
+        held[:, cols] = total.astype(bf16)
 
     def down_step(q, _):
-        for k in range(1, n - 1):
-
-            @pl.when(q == step_at(k))
-            def _():
-                w_step(2, k)
-
-        @pl.when(q < n)
-        def _():
-            weight = jnp.concatenate([down_full[:, cols] for cols in pieces(q)], axis=1)
-            for dx in others:
-                b = x_at(dx) + 1 - 2 * core
-                made = jnp.dot(hidden[rows(b), :], weight, preferred_element_type=f32)
-                gone(dx, q)[...] = made.astype(bf16)
-                made = jnp.dot(hidden[rows(x_at(dx)), :], weight, preferred_element_type=f32)
-                keep[dx, q] = made.astype(bf16)
-                pc_copy(dx, q).start()
-            for dx in range(1, nx):
-                pc_copy(dx, q).wait_recv()
-                both = keep[dx, q].astype(f32) + got_core[dx, q].astype(f32)
-                keep[dx, q] = both.astype(bf16)
-                px_copy(dx, q).start()
+        for at in range(n_piece - 2):
+            for k, ways in steps_before(at):
+
+                @pl.when(q == at)
+                def _():
+                    w_step(2, k, ways)
+
+        make_far(q)
+        make(q, 0)
+        pair_far(q)
 
         @pl.when(q > 1)
         def _():
-            p = q - 2
-            pc_copy(0, p).wait_recv()
-            total = keep[0, p].astype(f32) + got_core[0, p].astype(f32)
-            for dx in range(1, nx):
-                px_copy(dx, p).wait_recv()
-                total = total + got_x[dx - 1, p].astype(f32)
-            off = 0
-            for cols in pieces(p):
-                size = cols.size
-                whole = stream[:, cols].astype(f32) + total[:, off : off + size]
-                held[:, cols] = whole.astype(bf16)
-                off += size
+            finish(q - 2)
 
         return 0
 
-    lax.fori_loop(0, n + 2, down_step, 0)
+    lax.fori_loop(0, n_piece - 2, down_step, 0)
+    last = (n_piece - 2, n_piece - 1)
+    for q in last:
+        for k, ways in steps_before(q):
+            w_step(2, k, ways)
+        make_far(q)
+    for q in last:
+        pair_far(q)
+        make(q, 0)
+    for q in range(n_piece - 4, n_piece):
+        finish(q)
     sent(mix_full.at[pl.ds(0, nx * tok), :], p_send.at[0])
     for dx in range(1, nx):
         sent(mix_full.at[pl.ds(0, tok), :], p_send.at[1])
@@ -479,6 +503,8 @@
     ):
         tok, width = residual.shape
         depth, (hid, wide) = mixed.shape[1], down_weight.shape
+        piece = wide // 2 if wide % 256 == 0 else wide
+        n_piece = width // piece
         dma = pltpu.SemaphoreType.DMA
         whole = pl.BlockSpec(memory_space=pl.ANY)
         small = pl.BlockSpec(memory_space=pltpu.VMEM)
@@ -502,19 +528,20 @@
                 pltpu.VMEM((n_tp * tok, hid) if split else (8, 128), f32),
                 pltpu.VMEM((tok, depth), bf16),
                 pltpu.VMEM((tok, width), bf16),
-                pltpu.VMEM((nx, n_fs, tok, wide), bf16),
-                pltpu.VMEM((nx, n_fs, tok, wide), bf16),
-                pltpu.VMEM((max(nx - 1, 1), n_fs, tok, wide), bf16),
+                pltpu.VMEM((nx, n_piece, tok, piece), bf16),
+                pltpu.VMEM((nx, n_piece, tok, piece), bf16),
+                pltpu.VMEM((max(nx - 1, 1), n_piece, tok, piece), bf16),
                 dma((3,)),
                 dma((3, n_fs, 2)),
                 dma((3,)),
-                dma((n_fs, nx)),
-                dma((3,)),
+                dma((n_fs, 2)),
+                dma((n_fs, max(nx - 1, 1))),
+                dma((1,)),
                 dma((2,)),
                 dma((n_tp,)),
                 dma((2,)),
-                dma((n_fs, nx)),
-                dma((n_fs, max(nx - 1, 1))),
+                dma((n_piece, nx)),
+                dma((n_piece, max(nx - 1, 1))),
                 dma((6,)),
             ],
             compiler_params=pltpu.CompilerParams(

time: 197 us -> 195 us (0.990)
  no operation moved by 1% of the time
where the time goes in v3:
time: 195 us
  Pallas kernels  194 us (99%)
    pallas_call x1, Pallas kernels, body(): pl.pallas_call(functools.partial(layer_kernel, nz, ny, nx, split), out_sh...  194 us

profile of v3, /device:TPU:0, one launch (start us, length us, event | category | flops | bytes accessed | tf_op | source)
XLA Modules:
  0.0 195.0 jit_solution(17280983310803592387)
XLA Ops:
  0.0 193.9 %shard_map.91 = bf16[384,2048]{1,0:T(8,128)(2,1)S(1)} custom-call(bf16[384,2048]{1,0:T(8,128)(2,1)} %mixed.1, bf16[384,2048]{1,0:T(8,128)(2,1)} %residual.1, bf16[64,2048]{1,0:T(8,128)(2,1)} %mix_shard.1, bf16[1376,256]{1,0:T(8,128)(2,1)} %bitcast.3, bf16[1376,256]{1,0:T(8,128)(2,1)} %bitcast.4, bf16[1376,256]{1,0:T(8,128)(2,1)} %down_shard.1, ...), custom_call_target="tpu_custom_call" | custom-call | tf_op jit(solution)/shard_map/pallas_call | solution.py:515
  193.9 1.1 copy.11

commit v4 on v3

--- a/solution.py
+++ b/solution.py
@@ -46,10 +46,13 @@
     up_shard,
     gate_shard,
     down_shard,
+    gain_in,
+    taps_in,
+    bias_in,
+    held,
     gain,
     taps,
     bias,
-    held,
     mix_full,
     up_full,
     gate_full,
@@ -236,6 +239,10 @@
     load_mixed = pltpu.make_async_copy(mixed, mixed_v, in_sem.at[3])
     load_residual = pltpu.make_async_copy(residual, held, in_sem.at[4])
     load_mix = pltpu.make_async_copy(mix_shard, part(me, tp), in_sem.at[5])
+    small_loads = [
+        pltpu.make_async_copy(src, dst, in_sem.at[6 + i])
+        for i, (src, dst) in enumerate(((gain_in, gain), (taps_in, taps), (bias_in, bias)))
+    ]
 
     barrier = pltpu.get_barrier_semaphore()
     for other in (nxt, prv):
@@ -249,6 +256,8 @@
     load_mix.start()
     load_mixed.start()
     load_residual.start()
+    for load in small_loads:
+        load.start()
     for m in range(3):
         w_local(m).start()
     up_part[0:16, :] = jnp.zeros((16, hid), bf16)
@@ -268,6 +277,8 @@
     load_mix.wait()
     load_mixed.wait()
     load_residual.wait()
+    for load in small_loads:
+        load.wait()
 
     def project(i, _):
         cols = pl.ds(pl.multiple_of(i * TILE, 128), TILE)
@@ -515,9 +526,12 @@
         return pl.pallas_call(
             functools.partial(layer_kernel, nz, ny, nx, split),
             out_shape=pltpu.VMEM((tok, width), bf16),
-            in_specs=[whole] * 6 + [small] * 3,
+            in_specs=[whole] * 9,
             out_specs=small,
             scratch_shapes=[
+                pltpu.VMEM((1, width), f32),
+                pltpu.VMEM((3, hid), f32),
+                pltpu.VMEM((hid,), f32),
                 pltpu.VMEM((depth, width), bf16),
                 pltpu.VMEM((hid, width), bf16),
                 pltpu.VMEM((hid, width), bf16),
@@ -542,7 +556,7 @@
                 dma((2,)),
                 dma((n_piece, nx)),
                 dma((n_piece, max(nx - 1, 1))),
-                dma((6,)),
+                dma((9,)),
             ],
             compiler_params=pltpu.CompilerParams(
                 collective_id=0, has_side_effects=True, vmem_limit_bytes=VMEM - 2 * tok * width * 2

time: 195 us -> 194 us (level)
  no operation moved by 1% of the time
where the time goes in v4:
time: 194 us
  Pallas kernels  193 us (99%)
    pallas_call x1, Pallas kernels, body(): pl.pallas_call(functools.partial(layer_kernel, nz, ny, nx, split), out_sh...  193 us

profile of v4, /device:TPU:0, one launch (start us, length us, event | category | flops | bytes accessed | tf_op | source)
XLA Modules:
  0.0 194.2 jit_solution(7878750358289763329)
XLA Ops:
  0.0 193.1 %shard_map.91 = bf16[384,2048]{1,0:T(8,128)(2,1)S(1)} custom-call(bf16[384,2048]{1,0:T(8,128)(2,1)} %mixed.1, bf16[384,2048]{1,0:T(8,128)(2,1)} %residual.1, bf16[64,2048]{1,0:T(8,128)(2,1)} %mix_shard.1, bf16[1376,256]{1,0:T(8,128)(2,1)} %bitcast.3, bf16[1376,256]{1,0:T(8,128)(2,1)} %bitcast.4, bf16[1376,256]{1,0:T(8,128)(2,1)} %down_shard.1, ...), custom_call_target="tpu_custom_call" | custom-call | tf_op jit(solution)/shard_map/pallas_call | solution.py:526
  193.1 1.1 copy.11

commit v5 on v4

--- a/solution.py
+++ b/solution.py
@@ -69,7 +69,6 @@
     w_send,
     w_recv,
     m_send,
-    m_ring_recv,
     m_recv,
     m_core_recv,
     t_send,
@@ -136,7 +135,7 @@
         if mine:
             src = shards[m].at[:, at] if by_columns else shards[m].at[at, :]
         to = prv if way else nxt
-        return remote(src, slot(m, f, h), w_send.at[m], w_recv.at[m, f, h], "fs", to)
+        return remote(src, slot(m, f, h), w_send.at[m], w_recv.at[m % 2, f, h], "fs", to)
 
     def w_own(m):
         for k in range(2):
@@ -171,7 +170,7 @@
         if mine:
             src = mix_shard.at[:, pl.ds(*mix_cut[h])]
         to = prv if way else nxt
-        return remote(src, m_half(f, h), m_send.at[0], m_ring_recv.at[f, h], "fs", to)
+        return remote(src, m_half(f, h), m_send.at[0], w_recv.at[1, f, h], "fs", to)
 
     def m_x(f, dx, mine=False):
         src = mix_shard if mine else part(f, tp)
@@ -546,9 +545,8 @@
                 pltpu.VMEM((nx, n_piece, tok, piece), bf16),
                 pltpu.VMEM((max(nx - 1, 1), n_piece, tok, piece), bf16),
                 dma((3,)),
-                dma((3, n_fs, 2)),
+                dma((2, n_fs, 2)),
                 dma((3,)),
-                dma((n_fs, 2)),
                 dma((n_fs, max(nx - 1, 1))),
                 dma((1,)),
                 dma((2,)),

time: 194 us -> 194 us (level)
  no operation moved by 1% of the time
where the time goes in v5:
time: 194 us
  Pallas kernels  193 us (99%)
    pallas_call x1, Pallas kernels, body(): pl.pallas_call(functools.partial(layer_kernel, nz, ny, nx, split), out_sh...  193 us

profile of v5, /device:TPU:0, one launch (start us, length us, event | category | flops | bytes accessed | tf_op | source)
XLA Modules:
  0.0 193.9 jit_solution(4400324069362171682)
XLA Ops:
  0.0 192.8 %shard_map.91 = bf16[384,2048]{1,0:T(8,128)(2,1)S(1)} custom-call(bf16[384,2048]{1,0:T(8,128)(2,1)} %mixed.1, bf16[384,2048]{1,0:T(8,128)(2,1)} %residual.1, bf16[64,2048]{1,0:T(8,128)(2,1)} %mix_shard.1, bf16[1376,256]{1,0:T(8,128)(2,1)} %bitcast.3, bf16[1376,256]{1,0:T(8,128)(2,1)} %bitcast.4, bf16[1376,256]{1,0:T(8,128)(2,1)} %down_shard.1, ...), custom_call_target="tpu_custom_call" | custom-call | tf_op jit(solution)/shard_map/pallas_call | solution.py:525
  192.8 1.1 copy.11

commit v6 on v5

--- a/solution.py
+++ b/solution.py
@@ -75,6 +75,7 @@
     t_recv,
     p_send,
     pc_recv,
+    near_recv,
     px_recv,
     in_sem,
 ):
@@ -226,14 +227,21 @@
         at = pl.multiple_of(q * piece, 128)
         return mix_full.at[pl.ds(dx * tok, tok), pl.ds(at, piece)]
 
+    def pair_at(q):
+        if isinstance(q, int):
+            return q // 2 + (1 if q == n_piece - 1 else 0)
+        return lax.div(q, 2)
+
     def pc_copy(dx, q):
-        return remote(
-            gone(dx, q), got_core.at[dx, q], p_send.at[0], pc_recv.at[q, dx], "tp", twin
-        )
+        got = pc_recv.at[q, dx - 1] if dx else near_recv.at[pair_at(q)]
+        return remote(gone(dx, q), got_core.at[dx, q], p_send.at[0], got, "tp", twin)
 
     def px_copy(dx, q):
         src, dst = keep.at[dx, q], got_x.at[dx - 1, q]
-        return remote(src, dst, p_send.at[1], px_recv.at[q, dx - 1], "tp", x_at(dx))
+        return remote(src, dst, p_send.at[1], px_recv.at[pair_at(q), dx - 1], "tp", x_at(dx))
+
+    def wait_pieces(ref, got):
+        remote(ref, ref, p_send.at[0], got, "tp", twin).wait_recv()
 
     load_mixed = pltpu.make_async_copy(mixed, mixed_v, in_sem.at[3])
     load_residual = pltpu.make_async_copy(residual, held, in_sem.at[4])
@@ -452,15 +460,17 @@
             keep[dx, q] = both.astype(bf16)
             px_copy(dx, q).start()
 
-    def finish(q):
-        cols = piece_columns(q)
-        pc_copy(0, q).wait_recv()
-        total = stream[:, cols].astype(f32) + keep[0, q].astype(f32)
-        total = total + got_core[0, q].astype(f32)
+    def finish(q, count):
+        wait_pieces(got_core.at[0, pl.ds(q, count)], near_recv.at[pair_at(q)])
         for dx in range(1, nx):
-            px_copy(dx, q).wait_recv()
-            total = total + got_x[dx - 1, q].astype(f32)
-        held[:, cols] = total.astype(bf16)
+            wait_pieces(got_x.at[dx - 1, pl.ds(q, count)], px_recv.at[pair_at(q), dx - 1])
+        for i in range(count):
+            cols = piece_columns(q + i)
+            total = stream[:, cols].astype(f32) + keep[0, q + i].astype(f32)
+            total = total + got_core[0, q + i].astype(f32)
+            for dx in range(1, nx):
+                total = total + got_x[dx - 1, q + i].astype(f32)
+            held[:, cols] = total.astype(bf16)
 
     def down_step(q, _):
         for at in range(n_piece - 2):
@@ -474,9 +484,9 @@
         make(q, 0)
         pair_far(q)
 
-        @pl.when(q > 1)
+        @pl.when((q > 2) & (lax.rem(q, 2) == 1))
         def _():
-            finish(q - 2)
+            finish(q - 3, 2)
 
         return 0
 
@@ -489,8 +499,9 @@
     for q in last:
         pair_far(q)
         make(q, 0)
-    for q in range(n_piece - 4, n_piece):
-        finish(q)
+    finish(n_piece - 4, 2)
+    for q in last:
+        finish(q, 1)
     sent(mix_full.at[pl.ds(0, nx * tok), :], p_send.at[0])
     for dx in range(1, nx):
         sent(mix_full.at[pl.ds(0, tok), :], p_send.at[1])
@@ -552,8 +563,9 @@
                 dma((2,)),
                 dma((n_tp,)),
                 dma((2,)),
-                dma((n_piece, nx)),
                 dma((n_piece, max(nx - 1, 1))),
+                dma((n_piece // 2 + 1,)),
+                dma((n_piece // 2 + 1, max(nx - 1, 1))),
                 dma((9,)),
             ],
             compiler_params=pltpu.CompilerParams(

time: 194 us -> 194 us (level)
  no operation moved by 1% of the time
where the time goes in v6:
time: 194 us
  Pallas kernels  193 us (99%)
    pallas_call x1, Pallas kernels, body(): pl.pallas_call(functools.partial(layer_kernel, nz, ny, nx, split), out_sh...  193 us

profile of v6, /device:TPU:0, one launch (start us, length us, event | category | flops | bytes accessed | tf_op | source)
XLA Modules:
  0.0 193.8 jit_solution(2217598179474966498)
XLA Ops:
  0.0 192.7 %shard_map.91 = bf16[384,2048]{1,0:T(8,128)(2,1)S(1)} custom-call(bf16[384,2048]{1,0:T(8,128)(2,1)} %mixed.1, bf16[384,2048]{1,0:T(8,128)(2,1)} %residual.1, bf16[64,2048]{1,0:T(8,128)(2,1)} %mix_shard.1, bf16[1376,256]{1,0:T(8,128)(2,1)} %bitcast.3, bf16[1376,256]{1,0:T(8,128)(2,1)} %bitcast.4, bf16[1376,256]{1,0:T(8,128)(2,1)} %down_shard.1, ...), custom_call_target="tpu_custom_call" | custom-call | tf_op jit(solution)/shard_map/pallas_call | solution.py:536
  192.7 1.1 copy.11
